TPU v7x, 256 devices: a whole 4x4x8 slice. The times are simulated.
256 devices in a mesh: gr: 2 (over z_hi), fs: 16 (over z_lo, y), tp: 8 (over x, core).
Axes of the slice: x: 4, y: 4, z: 8 (z_hi: 2, z_lo: 4; z = z_hi * 4 + z_lo), core: 2. Of those that a mesh axis runs over, the one named last changes fastest.
Arguments:
- tokens: bfloat16 [8192, 2048], P(('gr', 'fs')), may hold values from -6 to 6
- route_ids: int32 [8192, 4], P(('gr', 'fs')), may hold values from 0 to 15, all different within a row; in each aligned block of 256 rows (0 to 255, 256 to 511, ...) at most 80 rows name the same one
- route_scores: float32 [8192, 4], P(('gr', 'fs')), may hold values from -4 to 4
- norm_gain: float32 [2048], P(('gr', 'fs')), may hold values from 0.1 to 1.9
- gate_weight: float32 [16, 2048, 2048], P(None, ('gr', 'fs'), 'tp'), may hold values from -0.5 to 0.5
- up_weight: float32 [16, 2048, 2048], P(None, ('gr', 'fs'), 'tp'), may hold values from -0.5 to 0.5
- down_weight: float32 [16, 2048, 2048], P(None, ('gr', 'fs'), 'tp'), may hold values from -0.03125 to 0.03125
Outputs:
- served_gate: bfloat16 [16, 2048, 2048], P('fs', None, 'tp')
- served_up: bfloat16 [16, 2048, 2048], P('fs', None, 'tp')
- served_down: bfloat16 [16, 2048, 2048], P('fs', None, 'tp')
- expert_mix: bfloat16 [8192, 2048], P(('gr', 'fs'), 'tp')
Inputs may be any that keep to these rules, and one draw needn't show every extreme that they name: `route_ids`: in each aligned block of 256 rows no expert is named by more than 80 pairs, and in some blocks one expert is named by exactly 80. The 4 experts of a token differ.
All inputs are finite; a program needn't handle non-finite values.
Results may differ from a plain program's by a relative error of at most 0.0092.
Values may be sent and summed in bfloat16 or wider, within the bound.
A program may use at most 64 MiB of HBM per device.

v0:
```python
import jax
import jax.numpy as jnp
from jax import lax
from jax.sharding import PartitionSpec as P

EXPERTS = 16
CAP = 80
norm_eps = 1e-06
clamp_limit = 7.0
sigmoid_slope = 1.702


def sent_together(arrays, axis, split_dim, concat_dim, along):
    ends, at = ([], 0)
    for a in arrays[:-1]:
        at += a.shape[along]
        ends.append(at)
    both = jnp.concatenate(arrays, axis=along)
    return tuple(
        jnp.split(
            lax.all_to_all(both, axis, split_axis=split_dim, concat_axis=concat_dim, tiled=True),
            ends,
            axis=along,
        )
    )


def laid_out(parts, dim):
    lengths = list(parts.shape[1:])
    lengths[dim] *= parts.shape[0]
    return jnp.moveaxis(parts, 0, dim).reshape(lengths)


def from_everyone(array, axis):
    devices = lax.axis_size(axis)
    return lax.all_to_all(
        jnp.broadcast_to(array[None], (devices, *array.shape)), axis, 0, 0, tiled=True
    )


def gathered_copies(array, axis, dim):
    return laid_out(from_everyone(array, axis), dim)


def side_by_side(arrays, axis, dim, along):
    widths = [a.shape[along] for a in arrays]
    both = jnp.concatenate(arrays, axis=along)
    filled = gathered_copies(both, axis, dim)
    return tuple(jnp.split(filled, [sum(widths[:k]) for k in range(1, len(widths))], axis=along))


def route_tables(block_ids, block_scores):
    row_count, top_count = block_ids.shape
    flattened = block_ids.reshape(-1)
    onehot = (flattened[:, None] == jnp.arange(EXPERTS, dtype=jnp.int32)[None, :]).astype(jnp.int32)
    before = jnp.cumsum(onehot, axis=0) - onehot
    slot_index = jnp.sum(before * onehot, axis=1)
    target = flattened * CAP + slot_index
    matches = (target[:, None] == jnp.arange(EXPERTS * CAP, dtype=jnp.int32)[None, :]).astype(
        jnp.float32
    )
    matches = matches.reshape(row_count, top_count, EXPERTS * CAP)
    exponent = jnp.exp(block_scores)
    weights = (exponent / jnp.sum(exponent, axis=1, keepdims=True)).astype(jnp.bfloat16)
    dispatch = jnp.sum(matches, axis=1).T.astype(jnp.bfloat16)
    combine = jnp.einsum("tk,tkc->tc", weights.astype(jnp.float32), matches).astype(jnp.bfloat16)
    return (dispatch, combine)


def activate(gate_pre, up_pre):
    clipped_gate = jnp.minimum(gate_pre, clamp_limit)
    clipped_up = jnp.clip(up_pre, -clamp_limit, clamp_limit)
    return (
        clipped_gate * jax.nn.sigmoid(sigmoid_slope * clipped_gate) * (clipped_up + 1.0)
    ).astype(jnp.bfloat16)


def local(tokens, route_ids, route_scores, norm_gain, gate_weight, up_weight, down_weight):
    scaling = norm_gain[None, :, None]
    folded = (
        (scaling * gate_weight).astype(jnp.bfloat16),
        (scaling * up_weight).astype(jnp.bfloat16),
        down_weight.astype(jnp.bfloat16),
    )
    by_expert = sent_together((folded[0], folded[1], folded[2]), "fs", 0, 1, 2)
    served_gate, served_up, served_down = side_by_side(
        (by_expert[0], by_expert[1], by_expert[2]), "gr", 1, 0
    )
    as_float = tokens.astype(jnp.float32)
    normed = (
        as_float * lax.rsqrt(jnp.mean(as_float * as_float, axis=1, keepdims=True) + norm_eps)
    ).astype(jnp.bfloat16)
    dispatch, combine = route_tables(route_ids, route_scores)
    column_width = normed.shape[1] // lax.axis_size("tp")
    normed = lax.dynamic_slice_in_dim(normed, lax.axis_index("tp") * column_width, column_width, 1)
    slot_rows = jnp.dot(dispatch, normed, preferred_element_type=jnp.float32).astype(jnp.bfloat16)
    outgoing = slot_rows.reshape(EXPERTS, 1, CAP, slot_rows.shape[1])
    portion = lax.all_gather(
        lax.all_to_all(outgoing, "fs", split_axis=0, concat_axis=1, tiled=True),
        "tp",
        axis=3,
        tiled=True,
    )
    gate_pre = jnp.einsum(
        "egnd,edf->egnf", portion, served_gate, preferred_element_type=jnp.float32
    )
    up_pre = jnp.einsum("egnd,edf->egnf", portion, served_up, preferred_element_type=jnp.float32)
    hidden = activate(gate_pre, up_pre)
    summed = jnp.einsum(
        "egnf,efd->egnd",
        lax.all_gather(hidden, "tp", axis=3, tiled=True),
        served_down,
        preferred_element_type=jnp.float32,
    )
    results = summed.astype(jnp.bfloat16)
    returned = lax.all_to_all(results, "fs", split_axis=1, concat_axis=0, tiled=True)
    flattened = returned.reshape(EXPERTS * CAP, returned.shape[3])
    expert_mix = jnp.dot(combine, flattened, preferred_element_type=jnp.float32).astype(
        jnp.bfloat16
    )
    return (served_gate, served_up, served_down, expert_mix)


def solution(mesh):
    in_specs = (
        P(("gr", "fs"), None),
        P(("gr", "fs"), None),
        P(("gr", "fs"), None),
        P(("gr", "fs")),
        P(None, ("gr", "fs"), "tp"),
        P(None, ("gr", "fs"), "tp"),
        P(None, ("gr", "fs"), "tp"),
    )
    out_specs = (
        P("fs", None, "tp"),
        P("fs", None, "tp"),
        P("fs", None, "tp"),
        P(("gr", "fs"), "tp"),
    )
    return jax.shard_map(local, mesh=mesh, in_specs=in_specs, out_specs=out_specs, check_vma=False)
```

profile of v0, /device:TPU:32, one launch (start us, length us, event | category | flops | bytes accessed | tf_op | source)
XLA Modules:
  0.0 250.1 jit_solution(6966143844637540849)
XLA Ops:
  7.2 0.0 all-gather.5.cloned.1.call-start
  7.2 0.8 copy.39
  8.0 0.1 eq.44
  8.2 0.1 eq.40
  8.3 0.0 copy-start
  8.3 1.5 convert_element_type.64
  9.8 0.0 copy-done
  9.9 0.0 copy-start.7
  9.9 0.3 multiply_reduce_fusion
  10.2 4.5 %reduce-window.6 = s32[16,8,128]{2,1,0:T(8,128)S(1)} reduce-window(s32[16,8,128]{2,1,0:T(8,128)S(1)} %fusion.29, s32[]{:T(128)} %constant.14.clone.1), window={size=1x1x128 pad=0_0x0_0x127_0}, to_apply=%region_1.0 | reduce-window | flops 2080768 | bytes 131076 | tf_op jit(solution)/shard_map/reduce-window
  14.7 0.1 slice.11
  14.8 0.1 copy.41
  14.9 0.1 copy.42
  15.0 0.1 broadcast_add_fusion
  15.1 0.1 reduce_sum.40
  15.3 0.1 copy.43
  15.3 0.0 copy-done.7
  15.4 0.8 convert_reduce_fusion
  16.2 0.4 convolution_convert_fusion
  16.6 0.0 copy-start.1
  16.6 0.0 copy-start.2
  16.6 0.0 copy-start.3
  16.6 0.0 copy-start.9
  16.7 26.7 %all_to_all.38 = bf16[16,1,80,256]{3,2,1,0:T(8,128)(2,1)} all-to-all(bf16[16,1,80,256]{3,2,1,0:T(8,128)(2,1)S(1)} %bitcast.70), channel_id=1, replica_groups=mesh['gr'=2,'fs'=16,'tp'=8] {'fs'}, dimensions={0} | all-to-all | bytes 1310720 | tf_op jit(solution)/shard_map/all_to_all | solution.py:99
  43.4 0.0 all-gather.5.cloned.1.call-update
  43.4 0.0 all-gather.7.cloned.1.call-start
  43.4 0.0 copy-done.1
  43.4 0.1 convert_element_type.57
  43.5 0.0 copy-done.2
  43.5 0.0 copy-done.3
  43.5 0.0 copy-done.9
  43.5 0.3 multiply_convert_fusion.1
  43.9 0.1 pad_maximum_fusion
  44.0 41.9 %all_to_all.39 = bf16[16,64,768]{2,1,0:T(8,128)(2,1)S(1)} all-to-all(bf16[16,64,768]{2,1,0:T(8,128)(2,1)S(1)} %pad_maximum_fusion), channel_id=1, replica_groups=mesh['gr'=2,'fs'=16,'tp'=8] {'fs'}, dimensions={0} | all-to-all | bytes 3145728 | tf_op jit(solution)/shard_map/all_to_all | solution.py:21
  85.9 0.1 fusion.33
  86.0 0.2 pad_maximum_fusion.1
  86.1 0.2 broadcast_in_dim.2
  86.4 77.5 %all_to_all.40 = bf16[2,3,1024,256]{3,2,1,0:T(8,128)(2,1)S(1)} all-to-all(bf16[2,3,1024,256]{3,2,1,0:T(8,128)(2,1)S(1)} %broadcast_in_dim.2), channel_id=1, replica_groups=mesh['gr'=2,'fs'=16,'tp'=8] {'gr'}, dimensions={0} | all-to-all | bytes 6291456 | tf_op jit(solution)/shard_map/all_to_all | solution.py:36
  163.8 0.2 fusion.32
  164.1 0.0 copy-start.6
  164.1 0.0 copy-start.5
  164.1 0.0 copy-start.4
  164.1 0.0 all-gather.5.cloned.1.call-done
  164.1 0.0 copy-start.10
  164.1 5.2 %fusion.9 = f32[16,80,256]{2,1,0:T(8,128)S(1)} fusion(bf16[2048,256,1]{1,0,2:T(8,128)(2,1)S(1)} %bitcast.76, bf16[16,1,80,2048]{3,2,0,1:T(8,128)(2,1)} %all-gather.5.cloned.1.call-done), kind=kOutput, calls=%fused_computation.13 | convolution fusion | flops 1342504960 | bytes 7602176 | tf_op jit(solution)/shard_map/egnd,edf->egnf/dot_general | solution.py:104
  169.3 0.0 copy-done.6
  169.3 0.0 copy-done.5
  169.3 0.0 copy-done.10
  169.3 2.7 %fusion.18 = bf16[16,80,256]{2,1,0:T(8,128)(2,1)} fusion(bf16[2048,256,1]{1,0,2:T(8,128)(2,1)S(1)} %bitcast.74, bf16[16,1,80,2048]{3,2,0,1:T(8,128)(2,1)S(1)} %copy-done.10, f32[16,80,256]{2,1,0:T(8,128)S(1)} %fusion.9), kind=kOutput, calls=%fused_computation.16 | convolution fusion | flops 1345126400 | bytes 8257536 | tf_op jit(solution)/shard_map/egnd,edf->egnf/dot_general | solution.py:107
  172.0 0.0 all-gather.7.cloned.1.call-update
  172.1 39.6 %all-gather.7.cloned.1.call-done = bf16[16,80,2048]{2,1,0:T(8,128)(2,1)} async-done(((bf16[16,80,256]{2,1,0:T(8,128)(2,1)}), bf16[16,80,2048]{2,1,0:T(8,128)(2,1)}) %all-gather.7.cloned.1.call-update) | async-done | bytes 5242896 | tf_op jit(solution)/shard_map/all_gather | solution.py:111
  211.7 0.0 copy-done.4
  211.7 0.0 copy-start.8
  211.7 4.9 %fusion.21 = bf16[1,16,80,256]{3,2,0,1:T(8,128)(2,1)} fusion(bf16[16,80,2048]{2,1,0:T(8,128)(2,1)} %all-gather.7.cloned.1.call-done, bf16[2048,256,1]{1,0,2:T(8,128)(2,1)S(1)} %bitcast.72), kind=kOutput, calls=%fused_computation.19 | convolution fusion | flops 1342504960 | bytes 6946816 | tf_op jit(solution)/shard_map/egnf,efd->egnd/dot_general | solution.py:109
  216.6 7.7 %all-to-all-start.3 = ((bf16[1,16,80,256]{3,2,0,1:T(8,128)(2,1)}), bf16[1,16,80,256]{3,2,0,1:T(8,128)(2,1)S(1)}, u32[]{:S(2)}, u32[]{:S(2)}) async-start(bf16[1,16,80,256]{3,2,0,1:T(8,128)(2,1)} %fusion.21), calls=%async_computation.3 | async-start | bytes 1310720 | tf_op jit(solution)/shard_map/all_to_all | solution.py:116
  224.4 0.0 copy-done.8
  224.4 0.2 copy.47
  224.6 0.8 iota_compare_fusion
  225.4 3.4 %fusion.4 = bf16[256,1,1280]{2,1,0:T(2,128)(2,1)S(1)} fusion(bf16[256,4,1]{1,2,0:T(2,128)(2,1)S(1)} %copy.47, pred[256,4,1280]{2,0,1:T(32,128)(4,1)S(1)} %iota_compare_fusion), kind=kOutput, calls=%fused_computation.6 | convolution fusion | flops 2621440 | bytes 1968128 | tf_op jit(solution)/shard_map/tk,tkc->tc/dot_general | solution.py:66
  228.8 13.5 %all-to-all-done.3 = bf16[1,16,80,256]{3,2,0,1:T(8,128)(2,1)S(1)} async-done(((bf16[1,16,80,256]{3,2,0,1:T(8,128)(2,1)}), bf16[1,16,80,256]{3,2,0,1:T(8,128)(2,1)S(1)}, u32[]{:S(2)}, u32[]{:S(2)}) %all-to-all-start.3) | async-done | bytes 655392 | tf_op jit(solution)/shard_map/all_to_all | solution.py:116
  242.3 1.0 convolution_convert_fusion.2
  (8 shorter events, 0.1 us)
Async XLA Ops:
  7.2 157.0 %all-gather.5.cloned.1.call-start = ((), (), s32[]{:S(2)}) async-start(), calls=%async_computation.4 | async-start | bytes 5898240 | tf_op jit(solution)/shard_map/all_gather | solution.py:98
  8.3 1.6 copy-start
  9.9 5.5 %copy-start.7 = (s32[256,4]{0,1:T(4,128)S(1)}, s32[256,4]{0,1:T(4,128)}, u32[]{:S(2)}) copy-start(s32[256,4]{0,1:T(4,128)} %param.8) | copy-start | bytes 12292
  16.6 26.8 %copy-start.1 = (f32[16,64,256]{2,1,0:T(8,128)S(1)}, f32[16,64,256]{2,1,0:T(8,128)}, u32[]{:S(2)}) copy-start(f32[16,64,256]{2,1,0:T(8,128)} %param.13) | copy-start | bytes 3145732
  16.6 26.9 %copy-start.2 = (f32[16,64,256]{2,1,0:T(8,128)S(1)}, f32[16,64,256]{2,1,0:T(8,128)}, u32[]{:S(2)}) copy-start(f32[16,64,256]{2,1,0:T(8,128)} %param.11) | copy-start | bytes 3145732
  16.6 26.9 %copy-start.3 = (f32[16,64,256]{2,1,0:T(8,128)S(1)}, f32[16,64,256]{2,1,0:T(8,128)}, u32[]{:S(2)}) copy-start(f32[16,64,256]{2,1,0:T(8,128)} %param.12) | copy-start | bytes 3145732
  16.6 26.9 %copy-start.9 = (f32[64]{0:T(128)S(1)}, f32[64]{0:T(128)}, u32[]{:S(2)}) copy-start(f32[64]{0:T(128)} %param.10) | copy-start | bytes 772
  43.4 168.3 %all-gather.7.cloned.1.call-start = ((), (), s32[]{:S(2)}) async-start(), calls=%async_computation.5 | async-start | bytes 5898240 | tf_op jit(solution)/shard_map/all_gather | solution.py:111
  164.1 5.3 %copy-start.6 = (bf16[1,2,1024,256]{3,2,0,1:T(8,128)(2,1)}, bf16[1,2,1024,256]{3,2,0,1:T(8,128)(2,1)S(1)}, u32[]{:S(2)}) copy-start(bf16[1,2,1024,256]{3,2,0,1:T(8,128)(2,1)S(1)} %get-tuple-element.6) | copy-start | bytes 3145732
  164.1 5.3 %copy-start.5 = (bf16[1,2,1024,256]{3,2,0,1:T(8,128)(2,1)}, bf16[1,2,1024,256]{3,2,0,1:T(8,128)(2,1)S(1)}, u32[]{:S(2)}) copy-start(bf16[1,2,1024,256]{3,2,0,1:T(8,128)(2,1)S(1)} %get-tuple-element.5) | copy-start | bytes 3145732
  164.1 47.6 %copy-start.4 = (bf16[1,2,1024,256]{3,2,0,1:T(8,128)(2,1)}, bf16[1,2,1024,256]{3,2,0,1:T(8,128)(2,1)S(1)}, u32[]{:S(2)}) copy-start(bf16[1,2,1024,256]{3,2,0,1:T(8,128)(2,1)S(1)} %get-tuple-element.4) | copy-start | bytes 3145732
  164.1 5.2 %copy-start.10 = (bf16[16,1,80,2048]{3,2,0,1:T(8,128)(2,1)S(1)}, bf16[16,1,80,2048]{3,2,0,1:T(8,128)(2,1)}, u32[]{:S(2)}) copy-start(bf16[16,1,80,2048]{3,2,0,1:T(8,128)(2,1)} %all-gather.5.cloned.1.call-done) | copy-start | bytes 15728644
  211.7 12.7 %copy-start.8 = (f32[256,4]{0,1:T(4,128)S(1)}, f32[256,4]{0,1:T(4,128)}, u32[]{:S(2)}) copy-start(f32[256,4]{0,1:T(4,128)} %param.9) | copy-start | bytes 12292
  216.6 25.7 %all-to-all-start.3 = ((bf16[1,16,80,256]{3,2,0,1:T(8,128)(2,1)}), bf16[1,16,80,256]{3,2,0,1:T(8,128)(2,1)S(1)}, u32[]{:S(2)}, u32[]{:S(2)}) async-start(bf16[1,16,80,256]{3,2,0,1:T(8,128)(2,1)} %fusion.21), calls=%async_computation.3 | async-start | bytes 1310720 | tf_op jit(solution)/shard_map/all_to_all | solution.py:116
Sparse Core Ops, SparseCore 0:
  43.5 41.8 all-gather.4
  172.2 39.4 all-gather.6
where the time goes:
time: 250 us
  blocking collectives  146 us (58%)
  waiting for transfers between devices  53.2 us (21%)
  matrix products  17.6 us (7%)
  between operations  14.4 us (6%)
  other arithmetic  8.79 us (4%)
  starting transfers between devices  7.83 us (3%)
    all_to_all x1, blocking collectives, from_everyone(): lax.all_to_all(jnp.broadcast_to(array[None], (devices, *array.shape)), ax...  77.5 us
    all_to_all x1, blocking collectives, sent_together(): lax.all_to_all(both, axis, split_axis=split_dim, concat_axis=concat_dim,...  41.9 us
    all_gather x1, waiting for transfers between devices, local(): lax.all_gather(hidden, 'tp', axis=3, tiled=True)  39.6 us
    all_to_all x1, blocking collectives, local(): lax.all_to_all(outgoing, 'fs', split_axis=0, concat_axis=1, tiled=True)  26.7 us
    all_to_all x1, waiting for transfers between devices, local(): lax.all_to_all(results, 'fs', split_axis=1, concat_axis=0, tiled=True)  13.5 us
    all_to_all x1, starting transfers between devices, local(): lax.all_to_all(results, 'fs', split_axis=1, concat_axis=0, tiled=True)  7.74 us
    dot_general x1, matrix products, local(): jnp.einsum('egnd,edf->egnf', portion, served_gate, preferred_element_type...  5.17 us
  transfers between devices with their start and end apart: 3, of which 2 were waited for; matrix products, arithmetic and copies ran while one was open for 2% of the time, Pallas kernels for 0%

commit v1 on v0

--- a/solution.py
+++ b/solution.py
@@ -8,6 +8,11 @@
 norm_eps = 1e-06
 clamp_limit = 7.0
 sigmoid_slope = 1.702
+
+
+def swapped_in(x, name, d):
+    sent = jnp.stack([x] * lax.axis_size(name))
+    return jnp.concatenate(lax.all_to_all(sent, name, 0, 0), axis=d)
 
 
 def sent_together(arrays, axis, split_dim, concat_dim, along):
@@ -108,7 +113,7 @@
     hidden = activate(gate_pre, up_pre)
     summed = jnp.einsum(
         "egnf,efd->egnd",
-        lax.all_gather(hidden, "tp", axis=3, tiled=True),
+        swapped_in(hidden, "tp", 3),
         served_down,
         preferred_element_type=jnp.float32,
     )

time: 250 us -> 287 us (1.15)
  blocking collectives: 146 us -> 211 us
  waiting for transfers between devices: 53.2 us -> 12.7 us
  local copies, waits for them, and re-layouts: 2.3 us -> 17 us
    all_to_all x0 -> x1, blocking collectives: none -> 65 us  [swapped_in(): return jnp.concatenate(lax.all_to_all(sent, name, 0, 0), axis=d)]
    all_gather x1 -> x0, waiting for transfers between devices: 39.6 us -> none  [local(): lax.all_gather(hidden, 'tp', axis=3, tiled=True)]
    another operation x2 -> x4, local copies, waits for them, and re-layouts: 0.08 us -> 9.42 us
    reshape x0 -> x1, local copies, waits for them, and re-layouts: none -> 5.37 us  [swapped_in(): return jnp.concatenate(lax.all_to_all(sent, name, 0, 0), axis=d)]
  transfers between devices with their start and end apart: 3 -> 2, of which waited for: 2 -> 1; matrix products, arithmetic and copies ran while one was open for 2% -> 2% of each run, Pallas kernels for 0% -> 0%
where the time goes in v1:
time: 287 us; the launch traced here: 286 us
  blocking collectives  211 us (74%)
  local copies, waits for them, and re-layouts  17 us (6%)
  matrix products  16.7 us (6%)
  between operations  14.4 us (5%)
  waiting for transfers between devices  12.7 us (4%)
  other arithmetic  8.79 us (3%)
  starting transfers between devices  5.64 us (2%)
    all_to_all x1, blocking collectives, from_everyone(): lax.all_to_all(jnp.broadcast_to(array[None], (devices, *array.shape)), ax...  77.5 us
    all_to_all x1, blocking collectives, swapped_in(): return jnp.concatenate(lax.all_to_all(sent, name, 0, 0), axis=d)  65 us
    all_to_all x1, blocking collectives, sent_together(): lax.all_to_all(both, axis, split_axis=split_dim, concat_axis=concat_dim,...  41.9 us
    all_to_all x1, blocking collectives, local(): lax.all_to_all(outgoing, 'fs', split_axis=0, concat_axis=1, tiled=True)  26.7 us
    all_to_all x1, waiting for transfers between devices, local(): lax.all_to_all(results, 'fs', split_axis=1, concat_axis=0, tiled=True)  12.7 us
    another operation x3, local copies, waits for them, and re-layouts  8.99 us
  transfers between devices with their start and end apart: 2, of which 1 were waited for; matrix products, arithmetic and copies ran while one was open for 2% of the time, Pallas kernels for 0%

profile of v1, /device:TPU:32, one launch (start us, length us, event | category | flops | bytes accessed | tf_op | source)
XLA Modules:
  0.0 286.3 jit_solution(1729131744597431133)
XLA Ops:
  7.2 0.0 all-gather.3.cloned.1.call-start
  7.2 0.8 copy.41
  8.0 0.1 eq.44
  8.2 0.1 eq.40
  8.3 0.0 copy-start
  8.3 1.5 convert_element_type.62
  9.8 0.0 copy-done
  9.9 0.0 copy-start.7
  9.9 0.3 multiply_reduce_fusion
  10.2 4.5 %reduce-window.6 = s32[16,8,128]{2,1,0:T(8,128)S(1)} reduce-window(s32[16,8,128]{2,1,0:T(8,128)S(1)} %fusion.29, s32[]{:T(128)} %constant.14.clone.1), window={size=1x1x128 pad=0_0x0_0x127_0}, to_apply=%region_1.0 | reduce-window | flops 2080768 | bytes 131076 | tf_op jit(solution)/shard_map/reduce-window
  14.7 0.1 slice.11
  14.8 0.1 copy.43
  14.9 0.1 copy.44
  15.0 0.1 broadcast_add_fusion
  15.1 0.1 reduce_sum.40
  15.3 0.1 copy.45
  15.3 0.0 copy-done.7
  15.4 0.8 convert_reduce_fusion
  16.2 0.4 convolution_convert_fusion
  16.6 0.0 copy-start.1
  16.6 0.0 copy-start.2
  16.6 0.0 copy-start.3
  16.6 0.0 copy-start.9
  16.7 26.7 %all_to_all.43 = bf16[16,1,80,256]{3,2,1,0:T(8,128)(2,1)} all-to-all(bf16[16,1,80,256]{3,2,1,0:T(8,128)(2,1)S(1)} %bitcast.74), channel_id=1, replica_groups=mesh['gr'=2,'fs'=16,'tp'=8] {'fs'}, dimensions={0} | all-to-all | bytes 1310720 | tf_op jit(solution)/shard_map/all_to_all | solution.py:104
  43.4 0.0 all-gather.3.cloned.1.call-update
  43.4 0.0 copy-done.1
  43.4 0.1 convert_element_type.55
  43.5 0.0 copy-done.2
  43.5 0.0 copy-done.3
  43.5 0.0 copy-done.9
  43.5 0.3 multiply_convert_fusion.1
  43.8 0.1 pad_maximum_fusion
  43.9 41.9 %all_to_all.44 = bf16[16,64,768]{2,1,0:T(8,128)(2,1)S(1)} all-to-all(bf16[16,64,768]{2,1,0:T(8,128)(2,1)S(1)} %pad_maximum_fusion), channel_id=1, replica_groups=mesh['gr'=2,'fs'=16,'tp'=8] {'fs'}, dimensions={0} | all-to-all | bytes 3145728 | tf_op jit(solution)/shard_map/all_to_all | solution.py:26
  85.8 0.1 fusion.33
  85.9 0.2 pad_maximum_fusion.1
  86.1 0.2 broadcast_in_dim.2
  86.3 77.5 %all_to_all.45 = bf16[2,3,1024,256]{3,2,1,0:T(8,128)(2,1)S(1)} all-to-all(bf16[2,3,1024,256]{3,2,1,0:T(8,128)(2,1)S(1)} %broadcast_in_dim.2), channel_id=1, replica_groups=mesh['gr'=2,'fs'=16,'tp'=8] {'gr'}, dimensions={0} | all-to-all | bytes 6291456 | tf_op jit(solution)/shard_map/all_to_all | solution.py:41
  163.8 0.2 fusion.32
  164.0 0.0 copy-start.6
  164.0 0.0 copy-start.5
  164.0 0.0 copy-start.4
  164.1 0.0 all-gather.3.cloned.1.call-done
  164.1 0.0 copy-start.10
  164.1 5.2 %fusion.9 = f32[16,80,256]{2,1,0:T(8,128)S(1)} fusion(bf16[2048,256,1]{1,0,2:T(8,128)(2,1)S(1)} %bitcast.80, bf16[16,1,80,2048]{3,2,0,1:T(8,128)(2,1)} %all-gather.3.cloned.1.call-done), kind=kOutput, calls=%fused_computation.13 | convolution fusion | flops 1342504960 | bytes 7602176 | tf_op jit(solution)/shard_map/egnd,edf->egnf/dot_general | solution.py:109
  169.3 0.0 copy-done.6
  169.3 0.0 copy-done.5
  169.3 0.0 copy-done.10
  169.3 1.8 fusion.18
  171.1 0.4 stack.2
  171.5 65.0 %all_to_all.46 = bf16[8,1,16,80,256]{4,3,2,1,0:T(8,128)(2,1)S(1)} all-to-all(bf16[8,1,16,80,256]{4,3,2,1,0:T(8,128)(2,1)S(1)} %stack.2), channel_id=1, replica_groups=mesh['gr'=2,'fs'=16,'tp'=8] {'tp'}, dimensions={0} | all-to-all | bytes 10485760 | tf_op jit(solution)/shard_map/all_to_all | solution.py:15
  236.6 5.4 %copy.48 = bf16[1,16,80,8,256]{4,3,2,1,0:T(8,128)(2,1)} copy(bf16[1,16,80,8,256]{4,2,1,0,3:T(8,128)(2,1)S(1)} %bitcast.71) | data formatting | bytes 10485760 | tf_op jit(solution)/shard_map/reshape | solution.py:15
  241.9 8.9 %reshape.130 = bf16[16,80,2048]{2,1,0:T(8,128)(2,1)} reshape(bf16[1,16,80,8,256]{4,3,2,1,0:T(8,128)(2,1)} %copy.48) | data formatting | bytes 10485760 | tf_op jit(solution)/shard_map/reshape.29
  250.8 0.0 copy-done.4
  250.8 0.0 copy-start.8
  250.8 4.9 %fusion.21 = bf16[1,16,80,256]{3,2,0,1:T(8,128)(2,1)} fusion(bf16[16,80,2048]{2,1,0:T(8,128)(2,1)} %reshape.130, bf16[2048,256,1]{1,0,2:T(8,128)(2,1)S(1)} %bitcast.76), kind=kOutput, calls=%fused_computation.19 | convolution fusion | flops 1342504960 | bytes 6946816 | tf_op jit(solution)/shard_map/egnf,efd->egnd/dot_general | solution.py:114
  255.7 5.6 %all-to-all-start.4 = ((bf16[1,16,80,256]{3,2,0,1:T(8,128)(2,1)}), bf16[1,16,80,256]{3,2,0,1:T(8,128)(2,1)S(1)}, u32[]{:S(2)}, u32[]{:S(2)}) async-start(bf16[1,16,80,256]{3,2,0,1:T(8,128)(2,1)} %fusion.21), calls=%async_computation.4 | async-start | bytes 1310720 | tf_op jit(solution)/shard_map/all_to_all | solution.py:121
  261.3 0.0 copy-done.8
  261.4 0.2 copy.50
  261.6 0.8 iota_compare_fusion
  262.4 3.4 %fusion.4 = bf16[256,1,1280]{2,1,0:T(2,128)(2,1)S(1)} fusion(bf16[256,4,1]{1,2,0:T(2,128)(2,1)S(1)} %copy.50, pred[256,4,1280]{2,0,1:T(32,128)(4,1)S(1)} %iota_compare_fusion), kind=kOutput, calls=%fused_computation.6 | convolution fusion | flops 2621440 | bytes 1968128 | tf_op jit(solution)/shard_map/tk,tkc->tc/dot_general | solution.py:71
  265.8 12.7 %all-to-all-done.4 = bf16[1,16,80,256]{3,2,0,1:T(8,128)(2,1)S(1)} async-done(((bf16[1,16,80,256]{3,2,0,1:T(8,128)(2,1)}), bf16[1,16,80,256]{3,2,0,1:T(8,128)(2,1)S(1)}, u32[]{:S(2)}, u32[]{:S(2)}) %all-to-all-start.4) | async-done | bytes 655392 | tf_op jit(solution)/shard_map/all_to_all | solution.py:121
  278.5 1.0 convolution_convert_fusion.2
  (8 shorter events, 0.1 us)
Async XLA Ops:
  7.2 156.9 %all-gather.3.cloned.1.call-start = ((), (), s32[]{:S(2)}) async-start(), calls=%async_computation.5 | async-start | bytes 5898240 | tf_op jit(solution)/shard_map/all_gather | solution.py:103
  8.3 1.6 copy-start
  9.9 5.5 %copy-start.7 = (s32[256,4]{0,1:T(4,128)S(1)}, s32[256,4]{0,1:T(4,128)}, u32[]{:S(2)}) copy-start(s32[256,4]{0,1:T(4,128)} %param.8) | copy-start | bytes 12292
  16.6 26.8 %copy-start.1 = (f32[16,64,256]{2,1,0:T(8,128)S(1)}, f32[16,64,256]{2,1,0:T(8,128)}, u32[]{:S(2)}) copy-start(f32[16,64,256]{2,1,0:T(8,128)} %param.13) | copy-start | bytes 3145732
  16.6 26.9 %copy-start.2 = (f32[16,64,256]{2,1,0:T(8,128)S(1)}, f32[16,64,256]{2,1,0:T(8,128)}, u32[]{:S(2)}) copy-start(f32[16,64,256]{2,1,0:T(8,128)} %param.11) | copy-start | bytes 3145732
  16.6 26.9 %copy-start.3 = (f32[16,64,256]{2,1,0:T(8,128)S(1)}, f32[16,64,256]{2,1,0:T(8,128)}, u32[]{:S(2)}) copy-start(f32[16,64,256]{2,1,0:T(8,128)} %param.12) | copy-start | bytes 3145732
  16.6 26.8 %copy-start.9 = (f32[64]{0:T(128)S(1)}, f32[64]{0:T(128)}, u32[]{:S(2)}) copy-start(f32[64]{0:T(128)} %param.10) | copy-start | bytes 772
  164.0 5.3 %copy-start.6 = (bf16[1,2,1024,256]{3,2,0,1:T(8,128)(2,1)}, bf16[1,2,1024,256]{3,2,0,1:T(8,128)(2,1)S(1)}, u32[]{:S(2)}) copy-start(bf16[1,2,1024,256]{3,2,0,1:T(8,128)(2,1)S(1)} %get-tuple-element.6) | copy-start | bytes 3145732
  164.0 5.3 %copy-start.5 = (bf16[1,2,1024,256]{3,2,0,1:T(8,128)(2,1)}, bf16[1,2,1024,256]{3,2,0,1:T(8,128)(2,1)S(1)}, u32[]{:S(2)}) copy-start(bf16[1,2,1024,256]{3,2,0,1:T(8,128)(2,1)S(1)} %get-tuple-element.5) | copy-start | bytes 3145732
  164.0 86.8 %copy-start.4 = (bf16[1,2,1024,256]{3,2,0,1:T(8,128)(2,1)}, bf16[1,2,1024,256]{3,2,0,1:T(8,128)(2,1)S(1)}, u32[]{:S(2)}) copy-start(bf16[1,2,1024,256]{3,2,0,1:T(8,128)(2,1)S(1)} %get-tuple-element.4) | copy-start | bytes 3145732
  164.1 5.2 %copy-start.10 = (bf16[16,1,80,2048]{3,2,0,1:T(8,128)(2,1)S(1)}, bf16[16,1,80,2048]{3,2,0,1:T(8,128)(2,1)}, u32[]{:S(2)}) copy-start(bf16[16,1,80,2048]{3,2,0,1:T(8,128)(2,1)} %all-gather.3.cloned.1.call-done) | copy-start | bytes 15728644
  250.8 10.5 %copy-start.8 = (f32[256,4]{0,1:T(4,128)S(1)}, f32[256,4]{0,1:T(4,128)}, u32[]{:S(2)}) copy-start(f32[256,4]{0,1:T(4,128)} %param.9) | copy-start | bytes 12292
  255.7 22.7 %all-to-all-start.4 = ((bf16[1,16,80,256]{3,2,0,1:T(8,128)(2,1)}), bf16[1,16,80,256]{3,2,0,1:T(8,128)(2,1)S(1)}, u32[]{:S(2)}, u32[]{:S(2)}) async-start(bf16[1,16,80,256]{3,2,0,1:T(8,128)(2,1)} %fusion.21), calls=%async_computation.4 | async-start | bytes 1310720 | tf_op jit(solution)/shard_map/all_to_all | solution.py:121
Sparse Core Ops, SparseCore 0:
  43.5 41.8 all-gather.2
